TPU v7x, 32 devices: a whole 2x2x4 slice. The times are simulated.
32 devices in a mesh: grp: 2 (over y), sp: 4 (over z), tp: 4 (over x, core).
Axes of the slice: x: 2, y: 2, z: 4, core: 2. Of those that a mesh axis runs over, the one named last changes fastest.
Arguments:
- stream: bfloat16 [6144, 4096], P(('grp', 'sp'), 'tp'), parts along dimension 0, may hold values from -400 to 400
- in_weight: bfloat16 [2, 1024, 4096], P(None, 'sp', 'tp'), may hold values from -0.09375 to 0.09375
- out_weight: bfloat16 [2, 1024, 4096], P(None, 'sp', 'tp'), may hold values from -0.1875 to 0.1875
- group_mix: bfloat16 [2, 4, 256, 256], replicated, may hold values from -0.375 to 0.375
- pool_gain: float32 [2, 1024], replicated, may hold values from 0.1 to 1.9
- norm_gain: float32 [2, 4096], P(None, 'tp'), may hold values from 0.1 to 1.9
- norm_shift: float32 [2, 4096], P(None, 'tp'), may hold values from -3 to 3
Outputs:
- refined: bfloat16 [6144, 4096], P(('grp', 'sp'), 'tp'), parts along dimension 0
There are 2 independent parts, one for each index of `grp`. A program takes and returns all parts, laid end to end along the dimension named above; an argument that names none is the same for every part. Nothing has to cross between parts.
All inputs are finite; a program needn't handle non-finite values.
Results may differ from a plain program's by a relative error of at most 0.015.
Values may be sent and summed in bfloat16 or wider, within the bound.
A program may use at most 64 MiB of HBM per device.

v0:
```python
import jax
import jax.numpy as jnp
from jax import lax
from jax.sharding import PartitionSpec as P

D = 4096
POOL = 1024
GROUPS = 4
GROUP_WIDTH = 256
LAYERS = 2
epsilon = 1e-05


def passed_along(block, axis, distance):
    devices = range(lax.axis_size(axis))
    route = [(i - distance, i) for i in devices if i - distance in devices]
    return lax.ppermute(block, axis, route)


def pooled_windows(hidden, tok_start):
    reach = 2**GROUPS - 1
    length = hidden.shape[1]
    channels = hidden.shape[0]
    earlier = passed_along(hidden[:, length - reach :], "sp", 1)
    extended = jnp.concatenate([earlier, hidden], axis=1).astype(jnp.float32)
    group_ids = (jnp.arange(channels, dtype=jnp.int32) // GROUP_WIDTH)[:, None]
    running = extended
    window_sums = jnp.zeros((channels, length), jnp.float32)
    for octave in range(GROUPS):
        offset = 2**octave
        running = running[:, offset:] + running[:, : running.shape[1] - offset]
        window_sums = jnp.where(
            group_ids == octave, running[:, running.shape[1] - length :], window_sums
        )
    positions = (tok_start + jnp.arange(length, dtype=jnp.int32) + 1).astype(jnp.float32)
    widths = jnp.exp2((group_ids + 1).astype(jnp.float32))
    counts = jnp.minimum(positions[None, :], widths)
    return (window_sums / counts - hidden.astype(jnp.float32)).astype(jnp.bfloat16)


def per_device(stream, in_weight, out_weight, group_mix, pool_gain, norm_gain, norm_shift):
    tok_rows = stream.shape[0]
    tok_start = lax.axis_index("sp") * tok_rows
    alpha = (2.0 * LAYERS) ** 0.25
    contract_rows = (((0,), (0,)), ((), ()))
    contract_cols = (((1,), (1,)), ((), ()))
    current = stream
    for layer_index in range(LAYERS):
        whole_in = lax.all_gather(in_weight[layer_index], "sp", axis=0, tiled=True)
        partial_value = lax.dot_general(
            whole_in, current, contract_cols, preferred_element_type=jnp.float32
        )
        hidden = lax.psum(partial_value.astype(jnp.bfloat16), "tp")
        pooled = pooled_windows(hidden, tok_start)
        grouped = pooled.reshape(GROUPS, GROUP_WIDTH, tok_rows)
        mixed = jnp.einsum(
            "gio,git->got", group_mix[layer_index], grouped, preferred_element_type=jnp.float32
        )
        gains = pool_gain[layer_index].reshape(GROUPS, GROUP_WIDTH, 1)
        scaled = (mixed * gains).astype(jnp.bfloat16).reshape(POOL, tok_rows)
        branch = lax.dot_general(
            scaled,
            lax.all_gather(out_weight[layer_index], "sp", axis=0, tiled=True),
            contract_rows,
            preferred_element_type=jnp.float32,
        )
        summed = alpha * current.astype(jnp.float32) + branch
        row_sum, row_squares = lax.psum(
            (jnp.sum(summed, axis=1), jnp.sum(summed * summed, axis=1)), "tp"
        )
        row_mean = row_sum / D
        row_var = row_squares / D - row_mean * row_mean
        normed = (summed - row_mean[:, None]) * lax.rsqrt(row_var + epsilon)[:, None]
        current = (
            normed * norm_gain[layer_index][None, :] + norm_shift[layer_index][None, :]
        ).astype(jnp.bfloat16)
    return current


def solution(mesh):
    in_specs = (
        P(("grp", "sp"), "tp"),
        P(None, "sp", "tp"),
        P(None, "sp", "tp"),
        P(),
        P(),
        P(None, "tp"),
        P(None, "tp"),
    )
    out_specs = P(("grp", "sp"), "tp")
    return jax.shard_map(
        per_device, mesh=mesh, in_specs=in_specs, out_specs=out_specs, check_vma=False
    )
```

profile of v0, /device:TPU:0, one launch (start us, length us, event | category | flops | bytes accessed | tf_op | source)
XLA Modules:
  0.0 312.8 jit_solution(13905823871252964514)
XLA Ops:
  6.5 0.0 all-gather.9.cloned.1.call-start
  6.5 2.2 fusion.49
  8.8 0.0 all-gather.9.cloned.1.call-update
  8.8 0.0 copy-start.2
  8.8 0.0 all-reduce.5.cloned.1.call-start
  8.9 48.5 %all-gather.9.cloned.1.call-done = bf16[1,1024,1024]{2,1,0:T(8,128)(2,1)} async-done(((bf16[1,256,1024]{2,1,0:T(8,128)(2,1)}), bf16[1,1024,1024]{2,1,0:T(8,128)(2,1)}) %all-gather.9.cloned.1.call-update) | async-done | bytes 2097168 | tf_op jit(solution)/shard_map/all_gather | solution.py:49
  57.3 5.0 %fusion.22 = bf16[1024,768]{1,0:T(8,128)(2,1)} fusion(bf16[768,1024]{1,0:T(8,128)(2,1)} %param.7, bf16[1,1024,1024]{2,1,0:T(8,128)(2,1)} %all-gather.9.cloned.1.call-done), kind=kOutput, calls=%fused_computation.40 | convolution fusion | flops 1611399168 | bytes 5242880 | tf_op jit(solution)/shard_map/dot_general | solution.py:50
  62.3 0.0 copy-start.4
  62.3 0.0 copy-start.5
  62.3 0.0 copy-start.6
  62.4 0.0 all-reduce.5.cloned.1.call-update
  62.4 0.0 all-gather.11.cloned.1.call-start
  62.4 0.0 copy-done.2
  62.4 1.1 fusion.48
  63.5 0.0 all-gather.11.cloned.1.call-update
  63.5 0.0 all-gather.13.cloned.1.call-start
  63.6 0.5 all-gather.13.cloned.1.call-update
  64.1 0.0 all-reduce.7.cloned.1.call-start
  64.2 0.0 copy-done.4
  64.3 0.0 copy-done.5
  64.3 0.0 copy-done.6
  64.3 39.9 %all-reduce.5.cloned.1.call-done = bf16[1024,768]{1,0:T(8,128)(2,1)} async-done(((bf16[1024,768]{1,0:T(8,128)(2,1)}), bf16[1024,768]{1,0:T(8,128)(2,1)}) %all-reduce.5.cloned.1.call-update) | async-done | bytes 1572880 | tf_op jit(solution)/shard_map/psum | solution.py:53
  104.2 1.1 slice.138
  105.3 3.4 %collective-permute-start = (bf16[1024,15]{1,0:T(8,128)(2,1)S(1)}, bf16[1024,15]{1,0:T(8,128)(2,1)S(1)}, u32[]{:S(2)}, u32[]{:S(2)}) collective-permute-start(bf16[1024,15]{1,0:T(8,128)(2,1)S(1)} %slice.138), channel_id=1, source_target_pairs={{0,4},{4,8},{8,12},{1,5},{5,9},{9,13},{2,6},{6,10},{10,14},{3,7},{... | collective-permute-start | bytes 92168 | tf_op jit(solution)/shard_map/ppermute | solution.py:17
  108.7 5.4 %collective-permute-done = bf16[1024,15]{1,0:T(8,128)(2,1)S(1)} collective-permute-done((bf16[1024,15]{1,0:T(8,128)(2,1)S(1)}, bf16[1024,15]{1,0:T(8,128)(2,1)S(1)}, u32[]{:S(2)}, u32[]{:S(2)}) %collective-permute-start) | collective-permute-done | bytes 30752 | tf_op jit(solution)/shard_map/ppermute | solution.py:17
  114.1 2.3 maximum_convert_fusion
  116.4 1.0 slice_add_fusion.5
  117.4 1.0 slice_add_fusion.4
  118.5 0.0 copy-start
  118.5 1.0 slice_add_fusion.3
  119.5 0.4 copy-done
  119.9 0.0 copy-start.3
  119.9 4.1 %fusion.1 = bf16[1024,768]{1,0:T(8,128)(2,1)S(1)} fusion(f32[1024,782]{1,0:T(8,128)S(1)} %slice_add_fusion.5, f32[1024,780]{1,0:T(8,128)S(1)} %slice_add_fusion.4, f32[1024,776]{1,0:T(8,128)S(1)} %slice_add_fusion.3, bf16[1024,768]{1,0:T(8,128)(2,1)S(1)} %copy-done, f32[1024]{0:T(1024)S(1)} %fusion.44, f32[768]{0:T(1024)S(1)} %add_convert_fusion.2, ...), kind=kLoop, calls=%fused_computation.9 | loop fusion | flops 7864320 | bytes 15739904 | tf_op jit(solution)/shard_map/convert_element_type | solution.py:38
  124.0 0.0 copy-done.3
  124.0 0.6 multiply_convert_fusion.1
  124.7 26.8 %all-gather.11.cloned.1.call-done = bf16[1,1024,1024]{2,1,0:T(8,128)(2,1)} async-done(((bf16[1,256,1024]{2,1,0:T(8,128)(2,1)}), bf16[1,1024,1024]{2,1,0:T(8,128)(2,1)}) %all-gather.11.cloned.1.call-update) | async-done | bytes 2097168 | tf_op jit(solution)/shard_map/all_gather | solution.py:63
  151.5 5.8 %fusion.47 = (f32[768]{0:T(1024)S(1)}, f32[768]{0:T(1024)S(1)}, f32[768,1024]{1,0:T(8,128)}) fusion(bf16[1024,768]{1,0:T(8,128)(2,1)S(1)} %bitcast.56, bf16[1,1024,1024]{2,1,0:T(8,128)(2,1)} %all-gather.11.cloned.1.call-done, bf16[768,1024]{1,0:T(8,128)(2,1)} %param.7), kind=kOutput, calls=%fused_computation.70 | convolution fusion | flops 1615329792 | bytes 8394752 | tf_op jit(solution)/shard_map/dot_general | solution.py:61
  157.3 6.5 %all-reduce.1 = (f32[768]{0:T(1024)S(1)}, f32[768]{0:T(1024)S(1)}) all-reduce(f32[768]{0:T(1024)S(1)} %get-tuple-element.8, f32[768]{0:T(1024)S(1)} %get-tuple-element.7), channel_id=1, replica_groups=mesh['grp'=2,'sp'=4,'tp'=4] {'tp'}, use_global_device_ids=true, to_apply=%region_4.5 | all-reduce | flops 1536 | bytes 12288 | tf_op jit(solution)/shard_map/psum | solution.py:68
  163.8 33.6 %all-gather.13.cloned.1.call-done = bf16[1,1024,1024]{2,1,0:T(8,128)(2,1)} async-done(((bf16[1,256,1024]{2,1,0:T(8,128)(2,1)}), bf16[1,1024,1024]{2,1,0:T(8,128)(2,1)}) %all-gather.13.cloned.1.call-update) | async-done | bytes 2097168 | tf_op jit(solution)/shard_map/all_gather | solution.py:49
  197.4 5.6 %fusion.28 = bf16[1024,768]{1,0:T(8,128)(2,1)} fusion(bf16[1,1024,1024]{2,1,0:T(8,128)(2,1)} %all-gather.13.cloned.1.call-done, f32[768,1024]{1,0:T(8,128)} %get-tuple-element.27, f32[1024]{0:T(1024)S(1)} %bitcast.61, f32[1024]{0:T(1024)S(1)} %bitcast.59, f32[768]{0:T(1024)S(1)} %get-tuple-element.26, f32[768]{0:T(1024)S(1)} %get-tuple-element.25), kind=kOutput, calls=%fused_computation.42 | convolution fusion | flops 1615331328 | bytes 6830080 | tf_op jit(solution)/shard_map/dot_general | solution.py:50
  203.1 0.0 all-reduce.7.cloned.1.call-update
  203.1 0.0 all-gather.15.cloned.1.call-start
  203.1 0.5 all-gather.15.cloned.1.call-update
  203.7 41.2 %all-reduce.7.cloned.1.call-done = bf16[1024,768]{1,0:T(8,128)(2,1)} async-done(((bf16[1024,768]{1,0:T(8,128)(2,1)}), bf16[1024,768]{1,0:T(8,128)(2,1)}) %all-reduce.7.cloned.1.call-update) | async-done | bytes 1572880 | tf_op jit(solution)/shard_map/psum | solution.py:53
  244.9 1.1 slice.149
  246.0 3.6 %collective-permute-start.1 = (bf16[1024,15]{1,0:T(8,128)(2,1)S(1)}, bf16[1024,15]{1,0:T(8,128)(2,1)S(1)}, u32[]{:S(2)}, u32[]{:S(2)}) collective-permute-start(bf16[1024,15]{1,0:T(8,128)(2,1)S(1)} %slice.149), channel_id=1, source_target_pairs={{0,4},{4,8},{8,12},{1,5},{5,9},{9,13},{2,6},{6,10},{10,14},{3,7},{... | collective-permute-start | bytes 92168 | tf_op jit(solution)/shard_map/ppermute | solution.py:17
  249.6 5.5 %collective-permute-done.1 = bf16[1024,15]{1,0:T(8,128)(2,1)S(1)} collective-permute-done((bf16[1024,15]{1,0:T(8,128)(2,1)S(1)}, bf16[1024,15]{1,0:T(8,128)(2,1)S(1)}, u32[]{:S(2)}, u32[]{:S(2)}) %collective-permute-start.1) | collective-permute-done | bytes 30752 | tf_op jit(solution)/shard_map/ppermute | solution.py:17
  255.2 2.2 maximum_convert_fusion.1
  257.4 1.0 slice_add_fusion.2
  258.4 1.0 slice_add_fusion.1
  259.4 0.0 copy-start.1
  259.4 1.0 slice_add_fusion
  260.5 0.4 copy-done.1
  260.9 4.1 %fusion.3 = bf16[1024,768]{1,0:T(8,128)(2,1)S(1)} fusion(f32[1024,782]{1,0:T(8,128)S(1)} %slice_add_fusion.2, f32[1024,780]{1,0:T(8,128)S(1)} %slice_add_fusion.1, f32[1024,776]{1,0:T(8,128)S(1)} %slice_add_fusion, bf16[1024,768]{1,0:T(8,128)(2,1)S(1)} %copy-done.1, f32[1024]{0:T(1024)S(1)} %fusion.44, f32[768]{0:T(1024)S(1)} %add_convert_fusion.2, ...), kind=kLoop, calls=%fused_computation.11 | loop fusion | flops 7864320 | bytes 15739904 | tf_op jit(solution)/shard_map/convert_element_type | solution.py:38
  265.0 1.8 multiply_convert_fusion
  266.8 25.3 %all-gather.15.cloned.1.call-done = bf16[1,1024,1024]{2,1,0:T(8,128)(2,1)} async-done(((bf16[1,256,1024]{2,1,0:T(8,128)(2,1)}), bf16[1,1024,1024]{2,1,0:T(8,128)(2,1)}) %all-gather.15.cloned.1.call-update) | async-done | bytes 2097168 | tf_op jit(solution)/shard_map/all_gather | solution.py:63
  292.1 5.6 %fusion.46 = (f32[768]{0:T(1024)S(1)}, f32[768]{0:T(1024)S(1)}, f32[768,1024]{1,0:T(8,128)S(1)}) fusion(bf16[1024,768]{1,0:T(8,128)(2,1)} %bitcast.55, bf16[1,1024,1024]{2,1,0:T(8,128)(2,1)} %all-gather.15.cloned.1.call-done, f32[1024]{0:T(1024)S(1)} %bitcast.62, f32[1024]{0:T(1024)S(1)} %bitcast.60, f32[768]{0:T(1024)S(1)} %get-tuple-element.26, ...), kind=kOutput, calls=%fused_computation.69 | convolution fusion | flops 1619261952 | bytes 9981952 | tf_op jit(solution)/shard_map/dot_general | solution.py:61
  297.7 6.5 %all-reduce = (f32[768]{0:T(1024)S(1)}, f32[768]{0:T(1024)S(1)}) all-reduce(f32[768]{0:T(1024)S(1)} %get-tuple-element.6, f32[768]{0:T(1024)S(1)} %get-tuple-element.5), channel_id=1, replica_groups=mesh['grp'=2,'sp'=4,'tp'=4] {'tp'}, use_global_device_ids=true, to_apply=%region_9.10 | all-reduce | flops 1536 | bytes 12288 | tf_op jit(solution)/shard_map/psum | solution.py:68
  304.2 1.7 add_convert_fusion
  (11 shorter events, 0.1 us)
Async XLA Ops:
  6.5 50.8 %all-gather.9.cloned.1.call-start = ((), (), s32[]{:S(2)}) async-start(), calls=%async_computation.2 | async-start | bytes 2621440 | tf_op jit(solution)/shard_map/all_gather | solution.py:49
  8.8 53.6 %copy-start.2 = (bf16[2,256,1024]{2,1,0:T(8,128)(2,1)S(1)}, bf16[2,256,1024]{2,1,0:T(8,128)(2,1)}, u32[]{:S(2)}) copy-start(bf16[2,256,1024]{2,1,0:T(8,128)(2,1)} %param.9) | copy-start | bytes 3145732
  8.8 95.4 %all-reduce.5.cloned.1.call-start = ((), (), s32[]{:S(2)}) async-start(), calls=%async_computation | async-start | bytes 3145728 | tf_op jit(solution)/shard_map/psum | solution.py:53
  62.3 1.9 copy-start.4
  62.3 1.9 copy-start.5
  62.3 1.9 copy-start.6
  62.4 89.1 %all-gather.11.cloned.1.call-start = ((), (), s32[]{:S(2)}) async-start(), calls=%async_computation.3 | async-start | bytes 2621440 | tf_op jit(solution)/shard_map/all_gather | solution.py:63
  63.5 133.9 %all-gather.13.cloned.1.call-start = ((), (), s32[]{:S(2)}) async-start(), calls=%async_computation.4 | async-start | bytes 2621440 | tf_op jit(solution)/shard_map/all_gather | solution.py:49
  64.1 180.8 %all-reduce.7.cloned.1.call-start = ((), (), s32[]{:S(2)}) async-start(), calls=%async_computation.1 | async-start | bytes 3145728 | tf_op jit(solution)/shard_map/psum | solution.py:53
  105.3 8.8 %collective-permute-start = (bf16[1024,15]{1,0:T(8,128)(2,1)S(1)}, bf16[1024,15]{1,0:T(8,128)(2,1)S(1)}, u32[]{:S(2)}, u32[]{:S(2)}) collective-permute-start(bf16[1024,15]{1,0:T(8,128)(2,1)S(1)} %slice.138), channel_id=1, source_target_pairs={{0,4},{4,8},{8,12},{1,5},{5,9},{9,13},{2,6},{6,10},{10,14},{3,7},{... | collective-permute-start | bytes 92168 | tf_op jit(solution)/shard_map/ppermute | solution.py:17
  118.5 1.4 copy-start
  119.9 4.1 %copy-start.3 = (bf16[2,4,256,256]{3,2,1,0:T(8,128)(2,1)S(1)}, bf16[2,4,256,256]{3,2,1,0:T(8,128)(2,1)}, u32[]{:S(2)}) copy-start(bf16[2,4,256,256]{3,2,1,0:T(8,128)(2,1)} %param.10) | copy-start | bytes 3145732
  203.1 89.0 %all-gather.15.cloned.1.call-start = ((), (), s32[]{:S(2)}) async-start(), calls=%async_computation.5 | async-start | bytes 2621440 | tf_op jit(solution)/shard_map/all_gather | solution.py:63
  246.0 9.2 %collective-permute-start.1 = (bf16[1024,15]{1,0:T(8,128)(2,1)S(1)}, bf16[1024,15]{1,0:T(8,128)(2,1)S(1)}, u32[]{:S(2)}, u32[]{:S(2)}) collective-permute-start(bf16[1024,15]{1,0:T(8,128)(2,1)S(1)} %slice.149), channel_id=1, source_target_pairs={{0,4},{4,8},{8,12},{1,5},{5,9},{9,13},{2,6},{6,10},{10,14},{3,7},{... | collective-permute-start | bytes 92168 | tf_op jit(solution)/shard_map/ppermute | solution.py:17
  259.4 1.4 copy-start.1
Sparse Core Ops, SparseCore 0:
  8.9 48.3 all-gather.8
  62.5 41.6 all-reduce.4
  105.8 45.7 all-gather.10
  152.9 44.4 all-gather.12
  203.2 41.6 all-reduce.6
  246.3 45.7 all-gather.14
where the time goes:
time: 313 us
  waiting for transfers between devices  227 us (73%)
  matrix products  24.5 us (8%)
  other arithmetic  20.6 us (7%)
  between operations  13.7 us (4%)
  blocking collectives  13 us (4%)
  starting transfers between devices  7.2 us (2%)
  local copies, waits for them, and re-layouts  6.35 us (2%)
    all_gather x2, waiting for transfers between devices, per_device(): whole_in = lax.all_gather(in_weight[layer_index], 'sp', axis=0, tiled=True)  82.1 us
    psum x2, waiting for transfers between devices, per_device(): hidden = lax.psum(partial_value.astype(jnp.bfloat16), 'tp')  81.1 us
    all_gather x2, waiting for transfers between devices, per_device(): lax.all_gather(out_weight[layer_index], 'sp', axis=0, tiled=True)  52.2 us
    psum x2, blocking collectives, per_device(): lax.psum((jnp.sum(summed, axis=1), jnp.sum(summed * summed, axis=1)), 'tp')  13 us
    dot_general x2, matrix products, per_device(): lax.dot_general(scaled, lax.all_gather(out_weight[layer_index], 'sp', axi...  11.4 us
    ppermute x2, waiting for transfers between devices, passed_along(): return lax.ppermute(block, axis, route)  10.9 us
    dot_general x2, matrix products, per_device(): lax.dot_general(whole_in, current, contract_cols, preferred_element_type=...  10.6 us
    convert_element_type x2, other arithmetic, pooled_windows(): (window_sums / counts - hidden.astype(jnp.float32)).astype(jnp.bfloat16)  8.26 us
  transfers between devices with their start and end apart: 8, of which 8 were waited for; matrix products, arithmetic and copies ran while one was open for 10% of the time, Pallas kernels for 0%

commit v1 on v0

--- a/solution.py
+++ b/solution.py
@@ -50,7 +50,9 @@
         partial_value = lax.dot_general(
             whole_in, current, contract_cols, preferred_element_type=jnp.float32
         )
-        hidden = lax.psum(partial_value.astype(jnp.bfloat16), "tp")
+        block_2 = partial_value.astype(jnp.bfloat16)
+        parts = lax.all_gather(block_2, "tp", axis=0, tiled=False)
+        hidden = parts.sum(axis=0)
         pooled = pooled_windows(hidden, tok_start)
         grouped = pooled.reshape(GROUPS, GROUP_WIDTH, tok_rows)
         mixed = jnp.einsum(

time: 313 us -> 330 us (1.054); the launches traced: 313 us -> 325 us
  other arithmetic: 20.6 us -> 33.9 us
  waiting for transfers between devices: 227 us -> 217 us
  local copies, waits for them, and re-layouts: 6.35 us -> 15.7 us
    all_gather x0 -> x2, waiting for transfers between devices: none -> 88.1 us  [per_device(): parts = lax.all_gather(block_2, 'tp', axis=0, tiled=False)]
    psum x2 -> x0, waiting for transfers between devices: 81.1 us -> none  [per_device(): hidden = lax.psum(partial_value.astype(jnp.bfloat16), 'tp')]
    all_gather x2, waiting for transfers between devices: 52.2 us -> 21.8 us  [per_device(): lax.all_gather(out_weight[layer_index], 'sp', axis=0, tiled=True)]
    reduce_sum x0 -> x2, other arithmetic: none -> 15.1 us  [per_device(): hidden = parts.sum(axis=0)]
    all_gather x0 -> x1, local copies, waits for them, and re-layouts: none -> 11.3 us  [per_device(): parts = lax.all_gather(block_2, 'tp', axis=0, tiled=False)]
    ppermute x2, waiting for transfers between devices: 10.9 us -> 21.7 us  [passed_along(): return lax.ppermute(block, axis, route)]
  transfers between devices with their start and end apart: 8 -> 8, of which waited for: 8 -> 8; matrix products, arithmetic and copies ran while one was open for 10% -> 17% of each run, Pallas kernels for 0% -> 0%
where the time goes in v1:
time: 330 us; the launch traced here: 325 us
  waiting for transfers between devices  217 us (66%)
  other arithmetic  33.9 us (10%)
  matrix products  24.4 us (7%)
  local copies, waits for them, and re-layouts  15.7 us (5%)
  between operations  13.7 us (4%)
  blocking collectives  12.6 us (4%)
  starting transfers between devices  7.72 us (2%)
    all_gather x2, waiting for transfers between devices, per_device(): parts = lax.all_gather(block_2, 'tp', axis=0, tiled=False)  88.1 us
    all_gather x2, waiting for transfers between devices, per_device(): whole_in = lax.all_gather(in_weight[layer_index], 'sp', axis=0, tiled=True)  84.7 us
    all_gather x2, waiting for transfers between devices, per_device(): lax.all_gather(out_weight[layer_index], 'sp', axis=0, tiled=True)  21.8 us
    ppermute x2, waiting for transfers between devices, passed_along(): return lax.ppermute(block, axis, route)  21.7 us
    reduce_sum x2, other arithmetic, per_device(): hidden = parts.sum(axis=0)  15.1 us
    psum x2, blocking collectives, per_device(): lax.psum((jnp.sum(summed, axis=1), jnp.sum(summed * summed, axis=1)), 'tp')  12.6 us
    dot_general x2, matrix products, per_device(): lax.dot_general(scaled, lax.all_gather(out_weight[layer_index], 'sp', axi...  11.4 us
    all_gather x1, local copies, waits for them, and re-layouts, per_device(): parts = lax.all_gather(block_2, 'tp', axis=0, tiled=False)  11.3 us
  transfers between devices with their start and end apart: 8, of which 8 were waited for; matrix products, arithmetic and copies ran while one was open for 17% of the time, Pallas kernels for 0%

profile of v1, /device:TPU:0, one launch (start us, length us, event | category | flops | bytes accessed | tf_op | source)
XLA Modules:
  0.0 325.4 jit_solution(9784226894225603617)
XLA Ops:
  6.5 0.0 all-gather.13.cloned.1.call-start
  6.5 2.3 fusion.49
  8.8 0.0 all-gather.13.cloned.1.call-update
  8.8 0.0 copy-start
  8.8 0.0 all-gather.15.cloned.1.call-start
  8.9 48.5 %all-gather.13.cloned.1.call-done = bf16[1,1024,1024]{2,1,0:T(8,128)(2,1)} async-done(((bf16[1,256,1024]{2,1,0:T(8,128)(2,1)}), bf16[1,1024,1024]{2,1,0:T(8,128)(2,1)}) %all-gather.13.cloned.1.call-update) | async-done | bytes 2097168 | tf_op jit(solution)/shard_map/all_gather | solution.py:49
  57.4 5.0 %fusion.22 = bf16[1024,768]{1,0:T(8,128)(2,1)} fusion(bf16[768,1024]{1,0:T(8,128)(2,1)} %param.7, bf16[1,1024,1024]{2,1,0:T(8,128)(2,1)} %all-gather.13.cloned.1.call-done), kind=kOutput, calls=%fused_computation.40 | convolution fusion | flops 1611399168 | bytes 5242880 | tf_op jit(solution)/shard_map/dot_general | solution.py:50
  62.4 0.0 copy-start.3
  62.4 0.0 copy-start.4
  62.4 0.0 copy-start.5
  62.4 0.0 all-gather.15.cloned.1.call-update
  62.4 0.0 all-gather.17.cloned.1.call-start
  62.4 0.0 copy-done
  62.5 1.1 fusion.48
  63.5 0.0 all-gather.17.cloned.1.call-update
  63.5 0.0 all-gather.19.cloned.1.call-start
  63.6 0.5 all-gather.19.cloned.1.call-update
  64.1 0.0 all-gather.21.cloned.1.call-start
  64.2 0.0 copy-done.3
  64.3 0.0 copy-done.4
  64.3 0.0 copy-done.5
  64.3 43.4 %all-gather.15.cloned.1.call-done = bf16[4096,768]{1,0:T(8,128)(2,1)} async-done(((bf16[1024,768]{1,0:T(8,128)(2,1)}), bf16[4096,768]{1,0:T(8,128)(2,1)}) %all-gather.15.cloned.1.call-update) | async-done | bytes 6291472 | tf_op jit(solution)/shard_map/all_gather | solution.py:54
  107.7 4.7 %reduce_sum.60 = bf16[1024,768]{1,0:T(8,128)(2,1)S(1)} reduce(bf16[4,1024,768]{2,1,0:T(8,128)(2,1)} %bitcast.56, bf16[]{:T(256)} %constant.51.clone.1), dimensions={0}, to_apply=%region_0.0 | reduce | flops 2359296 | bytes 7864322 | tf_op jit(solution)/shard_map/reduce_sum | solution.py:55
  112.4 0.1 slice.138
  112.6 3.4 %collective-permute-start = (bf16[1024,15]{1,0:T(8,128)(2,1)S(1)}, bf16[1024,15]{1,0:T(8,128)(2,1)S(1)}, u32[]{:S(2)}, u32[]{:S(2)}) collective-permute-start(bf16[1024,15]{1,0:T(8,128)(2,1)S(1)} %slice.138), channel_id=1, source_target_pairs={{0,4},{4,8},{8,12},{1,5},{5,9},{9,13},{2,6},{6,10},{10,14},{3,7},{... | collective-permute-start | bytes 92168 | tf_op jit(solution)/shard_map/ppermute | solution.py:17
  116.0 11.0 %collective-permute-done = bf16[1024,15]{1,0:T(8,128)(2,1)S(1)} collective-permute-done((bf16[1024,15]{1,0:T(8,128)(2,1)S(1)}, bf16[1024,15]{1,0:T(8,128)(2,1)S(1)}, u32[]{:S(2)}, u32[]{:S(2)}) %collective-permute-start) | collective-permute-done | bytes 30752 | tf_op jit(solution)/shard_map/ppermute | solution.py:17
  127.0 0.8 maximum_convert_fusion
  127.8 1.0 slice_add_fusion.5
  128.8 1.0 slice_add_fusion.4
  129.8 1.0 slice_add_fusion.3
  130.8 0.0 copy-start.1
  130.8 4.2 %fusion.1 = bf16[1024,768]{1,0:T(8,128)(2,1)S(1)} fusion(f32[1024,782]{1,0:T(8,128)S(1)} %slice_add_fusion.5, f32[1024,780]{1,0:T(8,128)S(1)} %slice_add_fusion.4, f32[1024,776]{1,0:T(8,128)S(1)} %slice_add_fusion.3, bf16[1024,768]{1,0:T(8,128)(2,1)S(1)} %reduce_sum.60, f32[1024]{0:T(1024)S(1)} %fusion.44, f32[768]{0:T(1024)S(1)} %add_convert_fusion.2, ...), kind=kLoop, calls=%fused_computation.9 | loop fusion | flops 7864320 | bytes 15739904 | tf_op jit(solution)/shard_map/convert_element_type | solution.py:38
  135.1 0.0 copy-done.1
  135.1 0.6 multiply_convert_fusion.1
  135.7 20.5 %all-gather.17.cloned.1.call-done = bf16[1,1024,1024]{2,1,0:T(8,128)(2,1)} async-done(((bf16[1,256,1024]{2,1,0:T(8,128)(2,1)}), bf16[1,1024,1024]{2,1,0:T(8,128)(2,1)}) %all-gather.17.cloned.1.call-update) | async-done | bytes 2097168 | tf_op jit(solution)/shard_map/all_gather | solution.py:65
  156.2 5.8 %fusion.47 = (f32[768]{0:T(1024)S(1)}, f32[768]{0:T(1024)S(1)}, f32[768,1024]{1,0:T(8,128)}) fusion(bf16[1024,768]{1,0:T(8,128)(2,1)S(1)} %bitcast.60, bf16[1,1024,1024]{2,1,0:T(8,128)(2,1)} %all-gather.17.cloned.1.call-done, bf16[768,1024]{1,0:T(8,128)(2,1)} %param.7), kind=kOutput, calls=%fused_computation.70 | convolution fusion | flops 1615329792 | bytes 8394752 | tf_op jit(solution)/shard_map/dot_general | solution.py:63
  162.0 6.2 %all-reduce.1 = (f32[768]{0:T(1024)S(1)}, f32[768]{0:T(1024)S(1)}) all-reduce(f32[768]{0:T(1024)S(1)} %get-tuple-element.8, f32[768]{0:T(1024)S(1)} %get-tuple-element.7), channel_id=1, replica_groups=mesh['grp'=2,'sp'=4,'tp'=4] {'tp'}, use_global_device_ids=true, to_apply=%region_4.5 | all-reduce | flops 1536 | bytes 12288 | tf_op jit(solution)/shard_map/psum | solution.py:70
  168.2 36.2 %all-gather.19.cloned.1.call-done = bf16[1,1024,1024]{2,1,0:T(8,128)(2,1)} async-done(((bf16[1,256,1024]{2,1,0:T(8,128)(2,1)}), bf16[1,1024,1024]{2,1,0:T(8,128)(2,1)}) %all-gather.19.cloned.1.call-update) | async-done | bytes 2097168 | tf_op jit(solution)/shard_map/all_gather | solution.py:49
  204.4 5.5 %fusion.28 = bf16[1024,768]{0,1:T(8,128)(2,1)} fusion(bf16[1,1024,1024]{2,1,0:T(8,128)(2,1)} %all-gather.19.cloned.1.call-done, f32[768,1024]{1,0:T(8,128)} %get-tuple-element.27, f32[1024]{0:T(1024)S(1)} %bitcast.65, f32[1024]{0:T(1024)S(1)} %bitcast.63, f32[768]{0:T(1024)S(1)} %get-tuple-element.26, f32[768]{0:T(1024)S(1)} %get-tuple-element.25), kind=kOutput, calls=%fused_computation.42 | convolution fusion | flops 1615331328 | bytes 6830080 | tf_op jit(solution)/shard_map/dot_general | solution.py:50
  210.0 0.0 all-gather.21.cloned.1.call-update
  210.0 0.0 all-gather.23.cloned.1.call-start
  210.0 0.5 all-gather.23.cloned.1.call-update
  210.6 44.7 %all-gather.21.cloned.1.call-done = bf16[4096,768]{0,1:T(8,128)(2,1)} async-done(((bf16[1024,768]{0,1:T(8,128)(2,1)}), bf16[4096,768]{0,1:T(8,128)(2,1)}) %all-gather.21.cloned.1.call-update) | async-done | bytes 6291472 | tf_op jit(solution)/shard_map/all_gather | solution.py:54
  255.3 11.3 %reshape.69 = bf16[4,1024,768]{1,0,2:T(4,128)(2,1)} reshape(bf16[4096,768]{0,1:T(8,128)(2,1)} %all-gather.21.cloned.1.call-done) | data formatting | bytes 12582912 | tf_op jit(solution)/shard_map/all_gather | solution.py:54
  266.5 10.4 %reduce_sum.63 = bf16[1024,768]{0,1:T(8,128)(2,1)S(1)} reduce(bf16[4,1024,768]{1,0,2:T(4,128)(2,1)} %reshape.69, bf16[]{:T(256)} %constant.51.clone.1), dimensions={0}, to_apply=%region_5.6 | reduce | flops 2359296 | bytes 7864322 | tf_op jit(solution)/shard_map/reduce_sum | solution.py:55
  277.0 0.2 copy.15
  277.2 4.1 %collective-permute-start.1 = (bf16[1024,15]{1,0:T(8,128)(2,1)S(1)}, bf16[1024,15]{1,0:T(8,128)(2,1)}, u32[]{:S(2)}, u32[]{:S(2)}) collective-permute-start(bf16[1024,15]{1,0:T(8,128)(2,1)S(1)} %copy.15), channel_id=1, source_target_pairs={{0,4},{4,8},{8,12},{1,5},{5,9},{9,13},{2,6},{6,10},{10,14},{3,7},{... | collective-permute-start | bytes 92168 | tf_op jit(solution)/shard_map/ppermute | solution.py:17
  281.3 0.7 copy.16
  282.0 10.7 %collective-permute-done.1 = bf16[1024,15]{1,0:T(8,128)(2,1)} collective-permute-done((bf16[1024,15]{1,0:T(8,128)(2,1)S(1)}, bf16[1024,15]{1,0:T(8,128)(2,1)}, u32[]{:S(2)}, u32[]{:S(2)}) %collective-permute-start.1) | collective-permute-done | bytes 30752 | tf_op jit(solution)/shard_map/ppermute | solution.py:17
  292.7 1.8 maximum_convert_fusion.1
  294.5 1.0 slice_add_fusion.2
  295.5 1.0 slice_add_fusion.1
  296.5 1.0 slice_add_fusion
  297.5 0.0 copy-start.2
  297.5 4.2 %fusion.3 = bf16[1024,768]{1,0:T(8,128)(2,1)S(1)} fusion(f32[1024,782]{1,0:T(8,128)S(1)} %slice_add_fusion.2, f32[1024,780]{1,0:T(8,128)S(1)} %slice_add_fusion.1, f32[1024,776]{1,0:T(8,128)S(1)} %slice_add_fusion, bf16[1024,768]{1,0:T(8,128)(2,1)S(1)} %copy.16, f32[1024]{0:T(1024)S(1)} %fusion.44, f32[768]{0:T(1024)S(1)} %add_convert_fusion.2, ...), kind=kLoop, calls=%fused_computation.11 | loop fusion | flops 7864320 | bytes 15739904 | tf_op jit(solution)/shard_map/convert_element_type | solution.py:38
  301.7 0.0 copy-done.2
  301.7 1.8 multiply_convert_fusion
  303.5 1.3 all-gather.23.cloned.1.call-done
  304.8 5.6 %fusion.46 = (f32[768]{0:T(1024)S(1)}, f32[768]{0:T(1024)S(1)}, f32[768,1024]{1,0:T(8,128)S(1)}) fusion(bf16[1024,768]{1,0:T(8,128)(2,1)} %bitcast.59, bf16[1,1024,1024]{2,1,0:T(8,128)(2,1)} %all-gather.23.cloned.1.call-done, f32[1024]{0:T(1024)S(1)} %bitcast.66, f32[1024]{0:T(1024)S(1)} %bitcast.64, f32[768]{0:T(1024)S(1)} %get-tuple-element.26, ...), kind=kOutput, calls=%fused_computation.69 | convolution fusion | flops 1619261952 | bytes 9981952 | tf_op jit(solution)/shard_map/dot_general | solution.py:63
  310.5 6.4 %all-reduce = (f32[768]{0:T(1024)S(1)}, f32[768]{0:T(1024)S(1)}) all-reduce(f32[768]{0:T(1024)S(1)} %get-tuple-element.6, f32[768]{0:T(1024)S(1)} %get-tuple-element.5), channel_id=1, replica_groups=mesh['grp'=2,'sp'=4,'tp'=4] {'tp'}, use_global_device_ids=true, to_apply=%region_9.10 | all-reduce | flops 1536 | bytes 12288 | tf_op jit(solution)/shard_map/psum | solution.py:70
  316.9 1.7 add_convert_fusion
  (12 shorter events, 0.1 us)
Async XLA Ops:
  6.5 50.8 %all-gather.13.cloned.1.call-start = ((), (), s32[]{:S(2)}) async-start(), calls=%async_computation | async-start | bytes 2621440 | tf_op jit(solution)/shard_map/all_gather | solution.py:49
  8.8 53.6 %copy-start = (bf16[2,256,1024]{2,1,0:T(8,128)(2,1)S(1)}, bf16[2,256,1024]{2,1,0:T(8,128)(2,1)}, u32[]{:S(2)}) copy-start(bf16[2,256,1024]{2,1,0:T(8,128)(2,1)} %param.9) | copy-start | bytes 3145732
  8.8 98.9 %all-gather.15.cloned.1.call-start = ((), (), s32[]{:S(2)}) async-start(), calls=%async_computation.1 | async-start | bytes 7864320 | tf_op jit(solution)/shard_map/all_gather | solution.py:54
  62.4 1.9 copy-start.3
  62.4 1.9 copy-start.4
  62.4 1.9 copy-start.5
  62.4 93.8 %all-gather.17.cloned.1.call-start = ((), (), s32[]{:S(2)}) async-start(), calls=%async_computation.2 | async-start | bytes 2621440 | tf_op jit(solution)/shard_map/all_gather | solution.py:65
  63.5 140.9 %all-gather.19.cloned.1.call-start = ((), (), s32[]{:S(2)}) async-start(), calls=%async_computation.3 | async-start | bytes 2621440 | tf_op jit(solution)/shard_map/all_gather | solution.py:49
  64.1 191.2 %all-gather.21.cloned.1.call-start = ((), (), s32[]{:S(2)}) async-start(), calls=%async_computation.4 | async-start | bytes 7864320 | tf_op jit(solution)/shard_map/all_gather | solution.py:54
  112.6 14.5 %collective-permute-start = (bf16[1024,15]{1,0:T(8,128)(2,1)S(1)}, bf16[1024,15]{1,0:T(8,128)(2,1)S(1)}, u32[]{:S(2)}, u32[]{:S(2)}) collective-permute-start(bf16[1024,15]{1,0:T(8,128)(2,1)S(1)} %slice.138), channel_id=1, source_target_pairs={{0,4},{4,8},{8,12},{1,5},{5,9},{9,13},{2,6},{6,10},{10,14},{3,7},{... | collective-permute-start | bytes 92168 | tf_op jit(solution)/shard_map/ppermute | solution.py:17
  130.8 4.2 %copy-start.1 = (bf16[2,4,256,256]{3,2,1,0:T(8,128)(2,1)S(1)}, bf16[2,4,256,256]{3,2,1,0:T(8,128)(2,1)}, u32[]{:S(2)}) copy-start(bf16[2,4,256,256]{3,2,1,0:T(8,128)(2,1)} %param.10) | copy-start | bytes 3145732
  210.0 94.8 %all-gather.23.cloned.1.call-start = ((), (), s32[]{:S(2)}) async-start(), calls=%async_computation.5 | async-start | bytes 2621440 | tf_op jit(solution)/shard_map/all_gather | solution.py:65
  277.2 15.5 %collective-permute-start.1 = (bf16[1024,15]{1,0:T(8,128)(2,1)S(1)}, bf16[1024,15]{1,0:T(8,128)(2,1)}, u32[]{:S(2)}, u32[]{:S(2)}) collective-permute-start(bf16[1024,15]{1,0:T(8,128)(2,1)S(1)} %copy.15), channel_id=1, source_target_pairs={{0,4},{4,8},{8,12},{1,5},{5,9},{9,13},{2,6},{6,10},{10,14},{3,7},{... | collective-permute-start | bytes 92168 | tf_op jit(solution)/shard_map/ppermute | solution.py:17
  297.5 4.2 %copy-start.2 = (bf16[2,4,256,256]{3,2,1,0:T(8,128)(2,1)S(1)}, bf16[2,4,256,256]{3,2,1,0:T(8,128)(2,1)}, u32[]{:S(2)}) copy-start(bf16[2,4,256,256]{3,2,1,0:T(8,128)(2,1)} %param.10) | copy-start | bytes 3145732
Sparse Core Ops, SparseCore 0:
  8.9 48.3 all-gather.12
  62.5 45.1 all-gather.14
  109.3 46.8 all-gather.16
  157.6 46.7 all-gather.18
  210.1 45.1 all-gather.20
  256.7 48.0 all-gather.22
